TPU v7x, 32 devices: a whole 2x2x4 slice. The times are simulated.
32 devices in a mesh: fs: 8 (over z, y), tp: 4 (over x, core).
Axes of the slice: x: 2, y: 2, z: 4, core: 2. Of those that a mesh axis runs over, the one named last changes fastest.
Arguments:
- resid: bfloat16 [8192, 2048], P(('fs', 'tp')), may hold values from -6 to 6
- mix_gain: float32 [2048], replicated, may hold values from 0.1 to 1.9
- w_query: bfloat16 [2048, 1024], P('fs', 'tp'), may hold values from -0.125 to 0.125
- w_key: bfloat16 [2048, 1024], P('fs', 'tp'), may hold values from -0.125 to 0.125
- w_value: bfloat16 [2048, 2048], P('fs', 'tp'), may hold values from -0.125 to 0.125
- w_gate: bfloat16 [2048, 2048], P('fs', 'tp'), may hold values from -0.125 to 0.125
- w_output: bfloat16 [2048, 2048], P('tp', 'fs'), may hold values from -0.125 to 0.125
- decay_rate: float32 [8], P('tp'), may hold values from 0.0008 to 0.034, as said below
- mlp_gain: float32 [2048], replicated, may hold values from 0.1 to 1.9
- w_up: bfloat16 [2048, 8192], P('fs', 'tp'), may hold values from -0.125 to 0.125
- w_down: bfloat16 [8192, 2048], P('tp', 'fs'), may hold values from -0.0625 to 0.0625
Outputs:
- layer_out: bfloat16 [8192, 2048], P(('fs', 'tp'))
Inputs may be any that keep to these rules, and one draw needn't show every extreme that they name: `decay_rate`: decay rates per position, one for each head.
All inputs are finite; a program needn't handle non-finite values.
Results may differ from a plain program's by a relative error of at most 0.038.
Values may be sent and summed in bfloat16 or wider, within the bound.
A program may use at most 64 MiB of HBM per device.

v0:
```python
import jax
import jax.numpy as jnp
from jax import lax
from jax.sharding import PartitionSpec as P

DK = 128
DV = 256
BLOCK = 128
LENGTH = 512
epsilon = 1e-06


def rms_scale(source, gains):
    widened = source.astype(jnp.float32)
    scaled = widened * lax.rsqrt(jnp.mean(widened * widened, axis=-1, keepdims=True) + epsilon)
    return (scaled * gains).astype(jnp.bfloat16)


def retention(queries, key_rows, values, rates):
    seq_count, length, head_count, key_width = queries.shape
    value_width = values.shape[-1]
    block_count = length // BLOCK
    queries = queries.reshape(seq_count, block_count, BLOCK, head_count, key_width)
    key_rows = key_rows.reshape(
        seq_count, block_count, BLOCK, head_count, key_width
    ) * key_width ** (-0.5)
    values = values.reshape(seq_count, block_count, BLOCK, head_count, value_width)
    places = jnp.arange(BLOCK, dtype=jnp.float32)
    offset = places[:, None] - places[None, :]
    causal = offset >= 0
    inner_decay = jnp.where(
        causal[None], jnp.exp(-rates[:, None, None] * jnp.where(causal, offset, 0.0)[None]), 0.0
    )
    scores = jnp.einsum("bnihd,bnjhd->bnhij", queries, key_rows) * inner_decay[None, None]
    within = jnp.einsum("bnhij,bnjhe->bnihe", scores, values)
    key_decayed = (
        key_rows
        * jnp.exp(-rates[None, :] * (BLOCK - 1.0 - places)[:, None])[None, None, :, :, None]
    )
    updates = jnp.einsum("bnjhd,bnjhe->nbhde", key_decayed, values)
    carry_decay = jnp.exp(-rates * BLOCK)[None, :, None, None]

    def advance(memory, update):
        return (carry_decay * memory + update, memory)

    _, before = lax.scan(
        advance, jnp.zeros((seq_count, head_count, key_width, value_width), jnp.float32), updates
    )
    query_decayed = (
        queries * jnp.exp(-rates[None, :] * (places + 1.0)[:, None])[None, None, :, :, None]
    )
    carried = jnp.einsum("bnihd,nbhde->bnihe", query_decayed, before)
    mixed = (within + carried).reshape(seq_count, length, head_count, value_width)
    centre = jnp.mean(mixed, axis=-1, keepdims=True)
    spread = jnp.mean(jnp.square(mixed - centre), axis=-1, keepdims=True)
    return (mixed - centre) * lax.rsqrt(spread + epsilon)


def heads_view(source, width):
    return source.astype(jnp.float32).reshape(-1, LENGTH, source.shape[1] // width, width)


def on_device(
    resid, mix_gain, w_query, w_key, w_value, w_gate, w_output, decay_rate, mlp_gain, w_up, w_down
):
    normed = lax.all_gather(rms_scale(resid, mix_gain), "tp", axis=0, tiled=True)
    tokens = normed.shape[0]
    pieces = (
        lax.all_gather(w_query, "fs", axis=0, tiled=True),
        lax.all_gather(w_key, "fs", axis=0, tiled=True),
        lax.all_gather(w_value, "fs", axis=0, tiled=True),
        lax.all_gather(w_gate, "fs", axis=0, tiled=True),
    )
    columns = normed
    projected = tuple(
        (jnp.dot(columns, shard_rows, preferred_element_type=jnp.float32) for shard_rows in pieces)
    )
    queries, key_rows, values, gate_rows = (
        member_sum.astype(jnp.bfloat16) for member_sum in projected
    )
    output_whole = lax.all_gather(w_output, "fs", axis=1, tiled=True)
    grouped = retention(
        heads_view(queries, DK), heads_view(key_rows, DK), heads_view(values, DV), decay_rate
    )
    gated = (jax.nn.silu(gate_rows.astype(jnp.float32)) * grouped.reshape(tokens, -1)).astype(
        jnp.bfloat16
    )
    mix_sum = lax.psum_scatter(
        jnp.dot(gated, output_whole, preferred_element_type=jnp.float32).astype(jnp.bfloat16),
        "tp",
        scatter_dimension=0,
        tiled=True,
    ).astype(jnp.float32)
    after_mix = (resid.astype(jnp.float32) + mix_sum).astype(jnp.bfloat16)
    normed_mlp = lax.all_gather(rms_scale(after_mix, mlp_gain), "tp", axis=0, tiled=True)
    columns = normed_mlp
    lifted = jnp.dot(
        columns, lax.all_gather(w_up, "fs", axis=0, tiled=True), preferred_element_type=jnp.float32
    )
    down_whole = lax.all_gather(w_down, "fs", axis=1, tiled=True)
    hidden = jnp.square(jax.nn.relu(lifted)).astype(jnp.bfloat16)
    mlp_sum = lax.psum_scatter(
        jnp.dot(hidden, down_whole, preferred_element_type=jnp.float32).astype(jnp.bfloat16),
        "tp",
        scatter_dimension=0,
        tiled=True,
    ).astype(jnp.float32)
    return (after_mix.astype(jnp.float32) + mlp_sum).astype(jnp.bfloat16)


def solution(mesh):
    placed = (
        P(("fs", "tp"), None),
        P(),
        P("fs", "tp"),
        P("fs", "tp"),
        P("fs", "tp"),
        P("fs", "tp"),
        P("tp", "fs"),
        P("tp"),
        P(),
        P("fs", "tp"),
        P("tp", "fs"),
    )
    return jax.shard_map(
        on_device, mesh=mesh, in_specs=placed, out_specs=P(("fs", "tp"), None), check_vma=False
    )
```

profile of v0, /device:TPU:0, one launch (start us, length us, event | category | flops | bytes accessed | tf_op | source)
XLA Modules:
  0.0 699.5 jit_solution(10212446089821985571)
XLA Ops:
  7.3 1.5 fusion.4
  8.8 2.5 fusion.6
  14.2 38.3 %all-gather.18.cloned.1.call-done = bf16[2048,256]{1,0:T(8,128)(2,1)} async-done(((bf16[256,256]{1,0:T(8,128)(2,1)}), bf16[2048,256]{1,0:T(8,128)(2,1)}) %all-gather.18.cloned.1.call-update) | async-done | bytes 1048592 | tf_op jit(solution)/shard_map/all_gather | solution.py:70
  52.5 34.8 %all-gather.10.cloned.1.call-done = bf16[1024,2048]{1,0:T(8,128)(2,1)} async-done(((bf16[256,2048]{1,0:T(8,128)(2,1)}), bf16[1024,2048]{1,0:T(8,128)(2,1)}) %all-gather.10.cloned.1.call-update) | async-done | bytes 4194320 | tf_op jit(solution)/shard_map/all_gather | solution.py:66
  87.2 3.7 fusion.13
  91.6 1.5 copy.28
  93.0 45.5 %all-gather.14.cloned.1.call-done = bf16[2048,512]{1,0:T(8,128)(2,1)} async-done(((bf16[256,512]{1,0:T(8,128)(2,1)}), bf16[2048,512]{1,0:T(8,128)(2,1)}) %all-gather.14.cloned.1.call-update) | async-done | bytes 2097168 | tf_op jit(solution)/shard_map/all_gather | solution.py:71
  138.5 5.2 convolution_convert_fusion.2
  143.7 1.1 reshape_reshape.15
  144.9 34.5 %all-gather.16.cloned.1.call-done = bf16[2048,256]{1,0:T(8,128)(2,1)} async-done(((bf16[256,256]{1,0:T(8,128)(2,1)}), bf16[2048,256]{1,0:T(8,128)(2,1)}) %all-gather.16.cloned.1.call-update) | async-done | bytes 1048592 | tf_op jit(solution)/shard_map/all_gather | solution.py:69
  179.3 3.7 convolution_convert_fusion.5
  184.0 2.0 fusion.14
  186.0 3.6 while.13
  189.6 3.4 fusion.17
  193.0 2.9 fusion.37
  195.9 2.4 copy.32
  198.8 1.2 mul.177
  200.4 1.2 sub.61
  201.7 1.6 copy.44
  204.0 1.5 copy.43
  205.5 23.6 %all-gather.12.cloned.1.call-done = bf16[2048,512]{1,0:T(8,128)(2,1)} async-done(((bf16[256,512]{1,0:T(8,128)(2,1)}), bf16[2048,512]{1,0:T(8,128)(2,1)}) %all-gather.12.cloned.1.call-update) | async-done | bytes 2097168 | tf_op jit(solution)/shard_map/all_gather | solution.py:72
  229.1 50.8 %all-gather.20.cloned.1.call-done = bf16[512,2048]{1,0:T(8,128)(2,1)} async-done(((bf16[512,256]{1,0:T(8,128)(2,1)}), bf16[512,2048]{1,0:T(8,128)(2,1)}) %all-gather.20.cloned.1.call-update) | async-done | bytes 2097168 | tf_op jit(solution)/shard_map/all_gather | solution.py:81
  279.9 11.3 %convolution_convert_fusion.1 = bf16[1024,2048]{1,0:T(8,128)(2,1)} fusion(bf16[512,2048]{1,0:T(8,128)(2,1)} %all-gather.20.cloned.1.call-done, f32[1024,512]{1,0:T(8,128)S(1)} %bitcast.46, f32[1024,512]{1,0:T(8,128)} %bitcast.48, f32[1024,512]{1,0:T(8,128)} %bitcast.47, bf16[1024,2048]{1,0:T(8,128)(2,1)} %all-gather.10.cloned.1.call-done, ...), kind=kOutput, calls=%fused_computation.4 | convolution fusion | flops 4302307328 | bytes 18874368 | tf_op jit(solution)/shard_map/dot_general | solution.py:89
  292.8 41.3 %reduce-scatter.3.cloned.1.call-done = bf16[256,2048]{1,0:T(8,128)(2,1)} async-done(((bf16[1024,2048]{1,0:T(8,128)(2,1)}), bf16[256,2048]{1,0:T(8,128)(2,1)}) %reduce-scatter.3.cloned.1.call-update) | async-done | bytes 1048592 | tf_op jit(solution)/shard_map/reduce_scatter | solution.py:88
  334.2 1.7 fusion.8
  336.0 1.5 fusion.10
  337.5 123.3 %all-gather.24.cloned.1.call-done = bf16[2048,2048]{1,0:T(8,128)(2,1)} async-done(((bf16[256,2048]{1,0:T(8,128)(2,1)}), bf16[2048,2048]{1,0:T(8,128)(2,1)}) %all-gather.24.cloned.1.call-update) | async-done | bytes 8388624 | tf_op jit(solution)/shard_map/all_gather | solution.py:98
  460.8 125.2 %all-gather.26.cloned.1.call-done = bf16[2048,2048]{1,0:T(8,128)(2,1)} async-done(((bf16[2048,256]{1,0:T(8,128)(2,1)}), bf16[2048,2048]{1,0:T(8,128)(2,1)}) %all-gather.26.cloned.1.call-update) | async-done | bytes 8388624 | tf_op jit(solution)/shard_map/all_gather | solution.py:100
  586.0 34.1 %all-gather.22.cloned.1.call-done = bf16[1024,2048]{1,0:T(8,128)(2,1)} async-done(((bf16[256,2048]{1,0:T(8,128)(2,1)}), bf16[1024,2048]{1,0:T(8,128)(2,1)}) %all-gather.22.cloned.1.call-update) | async-done | bytes 4194320 | tf_op jit(solution)/shard_map/all_gather | solution.py:95
  620.1 25.4 %convolution_convert_fusion = bf16[1024,2048]{1,0:T(8,128)(2,1)} fusion(bf16[2048,2048]{1,0:T(8,128)(2,1)} %all-gather.26.cloned.1.call-done, bf16[1024,2048]{1,0:T(8,128)(2,1)} %all-gather.22.cloned.1.call-done, bf16[2048,2048]{1,0:T(8,128)(2,1)} %all-gather.24.cloned.1.call-done), kind=kOutput, calls=%fused_computation.3 | convolution fusion | flops 17188257792 | bytes 25165824 | tf_op jit(solution)/shard_map/dot_general | solution.py:103
  645.5 44.8 %reduce-scatter.5.cloned.1.call-done = bf16[256,2048]{1,0:T(8,128)(2,1)} async-done(((bf16[1024,2048]{1,0:T(8,128)(2,1)}), bf16[256,2048]{1,0:T(8,128)(2,1)}) %reduce-scatter.5.cloned.1.call-update) | async-done | bytes 1048592 | tf_op jit(solution)/shard_map/reduce_scatter | solution.py:102
  690.3 2.7 fusion.11
  (62 shorter events, 11.7 us)
Async XLA Ops:
  6.5 46.0 %all-gather.18.cloned.1.call-start = ((), (), s32[]{:S(2)}) async-start(), calls=%async_computation.6 | async-start | bytes 1179648 | tf_op jit(solution)/shard_map/all_gather | solution.py:70
  7.3 80.0 %all-gather.10.cloned.1.call-start = ((), (), s32[]{:S(2)}) async-start(), calls=%async_computation.2 | async-start | bytes 5242880 | tf_op jit(solution)/shard_map/all_gather | solution.py:66
  8.8 5.2 copy-start.6
  11.4 127.1 %all-gather.14.cloned.1.call-start = ((), (), s32[]{:S(2)}) async-start(), calls=%async_computation.4 | async-start | bytes 2359296 | tf_op jit(solution)/shard_map/all_gather | solution.py:71
  12.1 167.2 %all-gather.16.cloned.1.call-start = ((), (), s32[]{:S(2)}) async-start(), calls=%async_computation.5 | async-start | bytes 1179648 | tf_op jit(solution)/shard_map/all_gather | solution.py:69
  12.7 216.4 %all-gather.12.cloned.1.call-start = ((), (), s32[]{:S(2)}) async-start(), calls=%async_computation.3 | async-start | bytes 2359296 | tf_op jit(solution)/shard_map/all_gather | solution.py:72
  13.3 266.6 %all-gather.20.cloned.1.call-start = ((), (), s32[]{:S(2)}) async-start(), calls=%async_computation.7 | async-start | bytes 2359296 | tf_op jit(solution)/shard_map/all_gather | solution.py:81
  13.9 320.3 %reduce-scatter.3.cloned.1.call-start = ((), (), s32[]{:S(2)}) async-start(), calls=%async_computation.8 | async-start | bytes 5242880 | tf_op jit(solution)/shard_map/reduce_scatter | solution.py:88
  91.5 52.2 %copy-start.2 = (f32[2,4,128,2,128]{4,3,2,1,0:T(2,128)}, f32[2,4,128,2,128]{4,3,2,1,0:T(2,128)S(1)}, u32[]{:S(2)}) copy-start(f32[2,4,128,2,128]{4,3,2,1,0:T(2,128)S(1)} %reshape.152) | copy-start | bytes 3145732
  189.6 3.4 copy-start.1
  201.7 2.3 copy-start.4
  291.3 42.9 %copy-start = (bf16[256,2048]{1,0:T(8,128)(2,1)S(1)}, bf16[256,2048]{1,0:T(8,128)(2,1)}, u32[]{:S(2)}) copy-start(bf16[256,2048]{1,0:T(8,128)(2,1)} %param.13) | copy-start | bytes 3145732
  291.3 44.6 %copy-start.5 = (f32[2048]{0:T(1024)S(1)}, f32[2048]{0:T(1024)}, u32[]{:S(2)}) copy-start(f32[2048]{0:T(1024)} %param.21) | copy-start | bytes 24580
  291.3 169.5 %all-gather.24.cloned.1.call-start = ((), (), s32[]{:S(2)}) async-start(), calls=%async_computation.10 | async-start | bytes 9437184 | tf_op jit(solution)/shard_map/all_gather | solution.py:98
  292.1 294.0 %all-gather.26.cloned.1.call-start = ((), (), s32[]{:S(2)}) async-start(), calls=%async_computation.11 | async-start | bytes 9437184 | tf_op jit(solution)/shard_map/all_gather | solution.py:100
  292.8 327.3 %all-gather.22.cloned.1.call-start = ((), (), s32[]{:S(2)}) async-start(), calls=%async_computation.9 | async-start | bytes 5242880 | tf_op jit(solution)/shard_map/all_gather | solution.py:95
  334.2 1.8 copy-start.3
  337.5 352.8 %reduce-scatter.5.cloned.1.call-start = ((), (), s32[]{:S(2)}) async-start(), calls=%async_computation.12 | async-start | bytes 5242880 | tf_op jit(solution)/shard_map/reduce_scatter | solution.py:102
Sparse Core Ops, SparseCore 0:
  9.5 42.9 all-gather.17
  54.0 33.1 all-gather.9
  89.4 49.0 all-gather.13
  140.5 38.7 all-gather.15
  181.3 47.7 all-gather.11
  231.0 48.8 all-gather.19
  291.4 42.7 reduce-scatter.2
  336.3 124.4 all-gather.23
  462.9 123.1 all-gather.25
  587.4 32.6 all-gather.21
  645.6 44.5 reduce-scatter.4
where the time goes:
time: 700 us
  waiting for transfers between devices  600 us (86%)
  matrix products  57.6 us (8%)
  other arithmetic  14 us (2%)
  local copies, waits for them, and re-layouts  13.5 us (2%)
  between operations  13.5 us (2%)
    all_gather x1, waiting for transfers between devices, on_device(): down_whole = lax.all_gather(w_down, 'fs', axis=1, tiled=True)  125 us
    all_gather x1, waiting for transfers between devices, on_device(): lax.all_gather(w_up, 'fs', axis=0, tiled=True)  123 us
    all_gather x1, waiting for transfers between devices, on_device(): output_whole = lax.all_gather(w_output, 'fs', axis=1, tiled=True)  50.8 us
    all_gather x1, waiting for transfers between devices, on_device(): lax.all_gather(w_value, 'fs', axis=0, tiled=True)  45.5 us
    reduce_scatter x1, waiting for transfers between devices, on_device(): lax.psum_scatter(jnp.dot(hidden, down_whole, preferred_element_type=jnp.f...  44.8 us
    reduce_scatter x1, waiting for transfers between devices, on_device(): lax.psum_scatter(jnp.dot(gated, output_whole, preferred_element_type=jnp....  41.3 us
    all_gather x1, waiting for transfers between devices, on_device(): lax.all_gather(w_key, 'fs', axis=0, tiled=True)  38.3 us
    all_gather x1, waiting for transfers between devices, on_device(): lax.all_gather(rms_scale(resid, mix_gain), 'tp', axis=0, tiled=True)  34.8 us
  transfers between devices with their start and end apart: 11, of which 11 were waited for; matrix products, arithmetic and copies ran while one was open for 6% of the time, Pallas kernels for 0%

commit v1 on v0

--- a/solution.py
+++ b/solution.py
@@ -78,7 +78,12 @@
     queries, key_rows, values, gate_rows = (
         member_sum.astype(jnp.bfloat16) for member_sum in projected
     )
-    output_whole = lax.all_gather(w_output, "fs", axis=1, tiled=True)
+    ring = [w_output]
+    for hop in range(7):
+        ring.append(lax.ppermute(ring[-1], "fs", [(dev, (dev + 1) % 8) for dev in range(8)]))
+    output_whole = jnp.roll(
+        jnp.concatenate(ring[::-1], axis=1), (lax.axis_index("fs") + 1) * ring[0].shape[1], axis=1
+    )
     grouped = retention(
         heads_view(queries, DK), heads_view(key_rows, DK), heads_view(values, DV), decay_rate
     )

time: 700 us -> 658 us (0.940)
  waiting for transfers between devices: 600 us -> 541 us
  local copies, waits for them, and re-layouts: 13.5 us -> 26 us
    ppermute x0 -> x7, waiting for transfers between devices: none -> 72 us  [on_device(): lax.ppermute(ring[-1], 'fs', [(dev, (dev + 1) % 8) for dev in range(8)])]
    all_gather x1 -> x0, waiting for transfers between devices: 50.8 us -> none  [on_device(): output_whole = lax.all_gather(w_output, 'fs', axis=1, tiled=True)]
    all_gather x1, waiting for transfers between devices: 38.3 us -> 0.01 us  [on_device(): lax.all_gather(w_key, 'fs', axis=0, tiled=True)]
    all_gather x1, waiting for transfers between devices: 34.8 us -> 0.01 us  [on_device(): lax.all_gather(rms_scale(resid, mix_gain), 'tp', axis=0, tiled=True)]
    unnamed x17 -> x34, local copies, waits for them, and re-layouts: 4.06 us -> 15.8 us
  transfers between devices with their start and end apart: 11 -> 17, of which waited for: 11 -> 15; matrix products, arithmetic and copies ran while one was open for 6% -> 9% of each run, Pallas kernels for 0% -> 0%
where the time goes in v1:
time: 658 us
  waiting for transfers between devices  541 us (82%)
  matrix products  58.2 us (9%)
  local copies, waits for them, and re-layouts  26 us (4%)
  other arithmetic  15 us (2%)
  between operations  13.7 us (2%)
    all_gather x1, waiting for transfers between devices, on_device(): down_whole = lax.all_gather(w_down, 'fs', axis=1, tiled=True)  125 us
    all_gather x1, waiting for transfers between devices, on_device(): lax.all_gather(w_up, 'fs', axis=0, tiled=True)  122 us
    ppermute x7, waiting for transfers between devices, on_device(): lax.ppermute(ring[-1], 'fs', [(dev, (dev + 1) % 8) for dev in range(8)])  72 us
    reduce_scatter x1, waiting for transfers between devices, on_device(): lax.psum_scatter(jnp.dot(hidden, down_whole, preferred_element_type=jnp.f...  44.8 us
    reduce_scatter x1, waiting for transfers between devices, on_device(): lax.psum_scatter(jnp.dot(gated, output_whole, preferred_element_type=jnp....  41.7 us
    all_gather x1, waiting for transfers between devices, on_device(): lax.all_gather(w_value, 'fs', axis=0, tiled=True)  40 us
    all_gather x1, waiting for transfers between devices, on_device(): lax.all_gather(w_query, 'fs', axis=0, tiled=True)  34.5 us
    all_gather x1, waiting for transfers between devices, on_device(): lax.all_gather(rms_scale(after_mix, mlp_gain), 'tp', axis=0, tiled=True)  34.2 us
  transfers between devices with their start and end apart: 17, of which 15 were waited for; matrix products, arithmetic and copies ran while one was open for 9% of the time, Pallas kernels for 0%

profile of v1, /device:TPU:0, one launch (start us, length us, event | category | flops | bytes accessed | tf_op | source)
XLA Modules:
  0.0 657.7 jit_solution(10302266576849519250)
XLA Ops:
  7.3 1.5 fusion.4
  8.8 2.5 fusion.6
  12.8 3.0 collective-permute-start
  15.8 9.5 %collective-permute-done = bf16[512,256]{1,0:T(8,128)(2,1)S(1)} collective-permute-done((bf16[512,256]{1,0:T(8,128)(2,1)S(1)}, bf16[512,256]{1,0:T(8,128)(2,1)S(1)}, u32[]{:S(2)}, u32[]{:S(2)}) %collective-permute-start) | collective-permute-done | bytes 262176 | tf_op jit(solution)/shard_map/ppermute | solution.py:83
  25.3 11.7 %collective-permute-done.1 = bf16[512,256]{1,0:T(8,128)(2,1)S(1)} collective-permute-done((bf16[512,256]{1,0:T(8,128)(2,1)S(1)}, bf16[512,256]{1,0:T(8,128)(2,1)S(1)}, u32[]{:S(2)}, u32[]{:S(2)}) %collective-permute-start.1) | collective-permute-done | bytes 262176 | tf_op jit(solution)/shard_map/ppermute | solution.py:83
  37.0 14.0 %collective-permute-done.2 = bf16[512,256]{1,0:T(8,128)(2,1)S(1)} collective-permute-done((bf16[512,256]{1,0:T(8,128)(2,1)S(1)}, bf16[512,256]{1,0:T(8,128)(2,1)S(1)}, u32[]{:S(2)}, u32[]{:S(2)}) %collective-permute-start.2) | collective-permute-done | bytes 262176 | tf_op jit(solution)/shard_map/ppermute | solution.py:83
  51.0 10.0 %collective-permute-done.3 = bf16[512,256]{1,0:T(8,128)(2,1)S(1)} collective-permute-done((bf16[512,256]{1,0:T(8,128)(2,1)S(1)}, bf16[512,256]{1,0:T(8,128)(2,1)S(1)}, u32[]{:S(2)}, u32[]{:S(2)}) %collective-permute-start.3) | collective-permute-done | bytes 262176 | tf_op jit(solution)/shard_map/ppermute | solution.py:83
  61.1 9.0 %collective-permute-done.4 = bf16[512,256]{1,0:T(8,128)(2,1)S(1)} collective-permute-done((bf16[512,256]{1,0:T(8,128)(2,1)S(1)}, bf16[512,256]{1,0:T(8,128)(2,1)S(1)}, u32[]{:S(2)}, u32[]{:S(2)}) %collective-permute-start.4) | collective-permute-done | bytes 262176 | tf_op jit(solution)/shard_map/ppermute | solution.py:83
  70.2 9.0 %collective-permute-done.5 = bf16[512,256]{1,0:T(8,128)(2,1)S(1)} collective-permute-done((bf16[512,256]{1,0:T(8,128)(2,1)S(1)}, bf16[512,256]{1,0:T(8,128)(2,1)S(1)}, u32[]{:S(2)}, u32[]{:S(2)}) %collective-permute-start.5) | collective-permute-done | bytes 262176 | tf_op jit(solution)/shard_map/ppermute | solution.py:83
  79.3 8.9 %collective-permute-done.6 = bf16[512,256]{1,0:T(8,128)(2,1)S(1)} collective-permute-done((bf16[512,256]{1,0:T(8,128)(2,1)S(1)}, bf16[512,256]{1,0:T(8,128)(2,1)S(1)}, u32[]{:S(2)}, u32[]{:S(2)}) %collective-permute-start.6) | collective-permute-done | bytes 262176 | tf_op jit(solution)/shard_map/ppermute | solution.py:83
  100.3 3.7 fusion.14
  106.1 40.0 %all-gather.13.cloned.1.call-done = bf16[2048,512]{1,0:T(8,128)(2,1)} async-done(((bf16[256,512]{1,0:T(8,128)(2,1)}), bf16[2048,512]{1,0:T(8,128)(2,1)}) %all-gather.13.cloned.1.call-update) | async-done | bytes 2097168 | tf_op jit(solution)/shard_map/all_gather | solution.py:71
  146.0 5.2 convolution_convert_fusion.2
  152.4 34.5 %all-gather.15.cloned.1.call-done = bf16[2048,256]{1,0:T(8,128)(2,1)} async-done(((bf16[256,256]{1,0:T(8,128)(2,1)}), bf16[2048,256]{1,0:T(8,128)(2,1)}) %all-gather.15.cloned.1.call-update) | async-done | bytes 1048592 | tf_op jit(solution)/shard_map/all_gather | solution.py:69
  186.9 3.7 convolution_convert_fusion.5
  191.6 2.0 fusion.15
  193.5 3.6 while.13
  197.1 3.3 fusion.18
  200.4 2.9 fusion.39
  203.4 2.3 copy.32
  207.5 1.5 copy.45
  213.4 23.2 %all-gather.11.cloned.1.call-done = bf16[2048,512]{1,0:T(8,128)(2,1)} async-done(((bf16[256,512]{1,0:T(8,128)(2,1)}), bf16[2048,512]{1,0:T(8,128)(2,1)}) %all-gather.11.cloned.1.call-update) | async-done | bytes 2097168 | tf_op jit(solution)/shard_map/all_gather | solution.py:72
  236.7 11.9 %convolution_convert_fusion.1 = bf16[1024,2048]{1,0:T(8,128)(2,1)} fusion(bf16[512,4096]{1,0:T(8,128)(2,1)} %constant_dynamic-update-slice_fusion, s32[]{:T(128)S(6)} %select_n.32, f32[1024,512]{1,0:T(8,128)} %bitcast.45, f32[1024,512]{1,0:T(8,128)} %bitcast.47, f32[1024,512]{1,0:T(8,128)} %bitcast.46, bf16[1024,2048]{1,0:T(8,128)(2,1)} %all-gather.9.cloned.1.call-done, ...), kind=kOutput, calls=%fused_computation.4 | convolution fusion | flops 4302307328 | bytes 18874372 | tf_op jit(solution)/shard_map/dot_general | solution.py:94
  250.2 41.7 %reduce-scatter.3.cloned.1.call-done = bf16[256,2048]{1,0:T(8,128)(2,1)} async-done(((bf16[1024,2048]{1,0:T(8,128)(2,1)}), bf16[256,2048]{1,0:T(8,128)(2,1)}) %reduce-scatter.3.cloned.1.call-update) | async-done | bytes 1048592 | tf_op jit(solution)/shard_map/reduce_scatter | solution.py:93
  291.9 1.6 fusion.8
  293.6 2.6 fusion.10
  296.2 122.3 %all-gather.21.cloned.1.call-done = bf16[2048,2048]{1,0:T(8,128)(2,1)} async-done(((bf16[256,2048]{1,0:T(8,128)(2,1)}), bf16[2048,2048]{1,0:T(8,128)(2,1)}) %all-gather.21.cloned.1.call-update) | async-done | bytes 8388624 | tf_op jit(solution)/shard_map/all_gather | solution.py:103
  418.5 125.2 %all-gather.23.cloned.1.call-done = bf16[2048,2048]{1,0:T(8,128)(2,1)} async-done(((bf16[2048,256]{1,0:T(8,128)(2,1)}), bf16[2048,2048]{1,0:T(8,128)(2,1)}) %all-gather.23.cloned.1.call-update) | async-done | bytes 8388624 | tf_op jit(solution)/shard_map/all_gather | solution.py:105
  543.7 34.2 %all-gather.19.cloned.1.call-done = bf16[1024,2048]{1,0:T(8,128)(2,1)} async-done(((bf16[256,2048]{1,0:T(8,128)(2,1)}), bf16[1024,2048]{1,0:T(8,128)(2,1)}) %all-gather.19.cloned.1.call-update) | async-done | bytes 4194320 | tf_op jit(solution)/shard_map/all_gather | solution.py:100
  577.9 25.4 %convolution_convert_fusion = bf16[1024,2048]{1,0:T(8,128)(2,1)} fusion(bf16[2048,2048]{1,0:T(8,128)(2,1)} %all-gather.23.cloned.1.call-done, bf16[1024,2048]{1,0:T(8,128)(2,1)} %all-gather.19.cloned.1.call-done, bf16[2048,2048]{1,0:T(8,128)(2,1)} %all-gather.21.cloned.1.call-done), kind=kOutput, calls=%fused_computation.3 | convolution fusion | flops 17188257792 | bytes 25165824 | tf_op jit(solution)/shard_map/dot_general | solution.py:108
  603.4 44.8 %reduce-scatter.5.cloned.1.call-done = bf16[256,2048]{1,0:T(8,128)(2,1)} async-done(((bf16[1024,2048]{1,0:T(8,128)(2,1)}), bf16[256,2048]{1,0:T(8,128)(2,1)}) %reduce-scatter.5.cloned.1.call-update) | async-done | bytes 1048592 | tf_op jit(solution)/shard_map/reduce_scatter | solution.py:107
  648.1 2.7 fusion.11
  (91 shorter events, 29.8 us)
Async XLA Ops:
  6.5 6.2 copy-start.5
  6.5 54.5 %copy-start.7 = (f32[2]{0:T(128)S(1)}, f32[2]{0:T(128)}, u32[]{:S(2)}) copy-start(f32[2]{0:T(128)} %param.20) | copy-start | bytes 28
  6.5 93.7 %all-gather.17.cloned.1.call-start = ((), (), s32[]{:S(2)}) async-start(), calls=%async_computation.6 | async-start | bytes 1179648 | tf_op jit(solution)/shard_map/all_gather | solution.py:70
  7.3 93.0 %all-gather.9.cloned.1.call-start = ((), (), s32[]{:S(2)}) async-start(), calls=%async_computation.2 | async-start | bytes 5242880 | tf_op jit(solution)/shard_map/all_gather | solution.py:66
  11.4 134.6 %all-gather.13.cloned.1.call-start = ((), (), s32[]{:S(2)}) async-start(), calls=%async_computation.4 | async-start | bytes 2359296 | tf_op jit(solution)/shard_map/all_gather | solution.py:71
  12.1 174.7 %all-gather.15.cloned.1.call-start = ((), (), s32[]{:S(2)}) async-start(), calls=%async_computation.5 | async-start | bytes 1179648 | tf_op jit(solution)/shard_map/all_gather | solution.py:69
  12.7 224.0 %all-gather.11.cloned.1.call-start = ((), (), s32[]{:S(2)}) async-start(), calls=%async_computation.3 | async-start | bytes 2359296 | tf_op jit(solution)/shard_map/all_gather | solution.py:72
  12.8 12.5 %collective-permute-start = (bf16[512,256]{1,0:T(8,128)(2,1)S(1)}, bf16[512,256]{1,0:T(8,128)(2,1)S(1)}, u32[]{:S(2)}, u32[]{:S(2)}) collective-permute-start(bf16[512,256]{1,0:T(8,128)(2,1)S(1)} %copy-done.5), channel_id=1, source_target_pairs={{0,4},{4,8},{8,12},{12,16},{16,20},{20,24},{24,28},{28,0},{1,5},{5... | collective-permute-start | bytes 786440 | tf_op jit(solution)/shard_map/ppermute | solution.py:83
  25.3 11.7 %collective-permute-start.1 = (bf16[512,256]{1,0:T(8,128)(2,1)S(1)}, bf16[512,256]{1,0:T(8,128)(2,1)S(1)}, u32[]{:S(2)}, u32[]{:S(2)}) collective-permute-start(bf16[512,256]{1,0:T(8,128)(2,1)S(1)} %collective-permute-done), channel_id=1, source_target_pairs={{0,4},{4,8},{8,12},{12,16},{16,20},{20,24},{24,28},{28,0},{1,5},{5... | collective-permute-start | bytes 786440 | tf_op jit(solution)/shard_map/ppermute | solution.py:83
  37.0 14.0 %collective-permute-start.2 = (bf16[512,256]{1,0:T(8,128)(2,1)S(1)}, bf16[512,256]{1,0:T(8,128)(2,1)S(1)}, u32[]{:S(2)}, u32[]{:S(2)}) collective-permute-start(bf16[512,256]{1,0:T(8,128)(2,1)S(1)} %collective-permute-done.1), channel_id=1, source_target_pairs={{0,4},{4,8},{8,12},{12,16},{16,20},{20,24},{24,28},{28,0},{1,5},{5... | collective-permute-start | bytes 786440 | tf_op jit(solution)/shard_map/ppermute | solution.py:83
  51.0 10.1 %collective-permute-start.3 = (bf16[512,256]{1,0:T(8,128)(2,1)S(1)}, bf16[512,256]{1,0:T(8,128)(2,1)S(1)}, u32[]{:S(2)}, u32[]{:S(2)}) collective-permute-start(bf16[512,256]{1,0:T(8,128)(2,1)S(1)} %collective-permute-done.2), channel_id=1, source_target_pairs={{0,4},{4,8},{8,12},{12,16},{16,20},{20,24},{24,28},{28,0},{1,5},{5... | collective-permute-start | bytes 786440 | tf_op jit(solution)/shard_map/ppermute | solution.py:83
  51.0 240.9 %reduce-scatter.3.cloned.1.call-start = ((), (), s32[]{:S(2)}) async-start(), calls=%async_computation.7 | async-start | bytes 5242880 | tf_op jit(solution)/shard_map/reduce_scatter | solution.py:93
  61.0 9.1 %collective-permute-start.4 = (bf16[512,256]{1,0:T(8,128)(2,1)S(1)}, bf16[512,256]{1,0:T(8,128)(2,1)S(1)}, u32[]{:S(2)}, u32[]{:S(2)}) collective-permute-start(bf16[512,256]{1,0:T(8,128)(2,1)S(1)} %collective-permute-done.3), channel_id=1, source_target_pairs={{0,4},{4,8},{8,12},{12,16},{16,20},{20,24},{24,28},{28,0},{1,5},{5... | collective-permute-start | bytes 786440 | tf_op jit(solution)/shard_map/ppermute | solution.py:83
  70.1 9.1 %collective-permute-start.5 = (bf16[512,256]{1,0:T(8,128)(2,1)S(1)}, bf16[512,256]{1,0:T(8,128)(2,1)S(1)}, u32[]{:S(2)}, u32[]{:S(2)}) collective-permute-start(bf16[512,256]{1,0:T(8,128)(2,1)S(1)} %collective-permute-done.4), channel_id=1, source_target_pairs={{0,4},{4,8},{8,12},{12,16},{16,20},{20,24},{24,28},{28,0},{1,5},{5... | collective-permute-start | bytes 786440 | tf_op jit(solution)/shard_map/ppermute | solution.py:83
  79.1 9.1 %collective-permute-start.6 = (bf16[512,256]{1,0:T(8,128)(2,1)S(1)}, bf16[512,256]{1,0:T(8,128)(2,1)S(1)}, u32[]{:S(2)}, u32[]{:S(2)}) collective-permute-start(bf16[512,256]{1,0:T(8,128)(2,1)S(1)} %collective-permute-done.5), channel_id=1, source_target_pairs={{0,4},{4,8},{8,12},{12,16},{16,20},{20,24},{24,28},{28,0},{1,5},{5... | collective-permute-start | bytes 786440 | tf_op jit(solution)/shard_map/ppermute | solution.py:83
  104.6 46.7 %copy-start.2 = (f32[2,4,128,2,128]{4,3,2,1,0:T(2,128)}, f32[2,4,128,2,128]{4,3,2,1,0:T(2,128)S(1)}, u32[]{:S(2)}) copy-start(f32[2,4,128,2,128]{4,3,2,1,0:T(2,128)S(1)} %reshape.152) | copy-start | bytes 3145732
  197.1 3.4 copy-start.1
  209.0 3.0 copy-start.4
  248.6 43.3 %copy-start = (bf16[256,2048]{1,0:T(8,128)(2,1)S(1)}, bf16[256,2048]{1,0:T(8,128)(2,1)}, u32[]{:S(2)}) copy-start(bf16[256,2048]{1,0:T(8,128)(2,1)} %param.13) | copy-start | bytes 3145732
  248.6 45.0 %copy-start.6 = (f32[2048]{0:T(1024)S(1)}, f32[2048]{0:T(1024)}, u32[]{:S(2)}) copy-start(f32[2048]{0:T(1024)} %param.21) | copy-start | bytes 24580
  248.6 169.9 %all-gather.21.cloned.1.call-start = ((), (), s32[]{:S(2)}) async-start(), calls=%async_computation.9 | async-start | bytes 9437184 | tf_op jit(solution)/shard_map/all_gather | solution.py:103
  249.4 294.3 %all-gather.23.cloned.1.call-start = ((), (), s32[]{:S(2)}) async-start(), calls=%async_computation.10 | async-start | bytes 9437184 | tf_op jit(solution)/shard_map/all_gather | solution.py:105
  250.1 327.8 %all-gather.19.cloned.1.call-start = ((), (), s32[]{:S(2)}) async-start(), calls=%async_computation.8 | async-start | bytes 5242880 | tf_op jit(solution)/shard_map/all_gather | solution.py:100
  296.2 351.9 %reduce-scatter.5.cloned.1.call-start = ((), (), s32[]{:S(2)}) async-start(), calls=%async_computation.11 | async-start | bytes 5242880 | tf_op jit(solution)/shard_map/reduce_scatter | solution.py:107
  603.3 44.8 %copy-start.3 = (bf16[256,2048]{1,0:T(8,128)(2,1)S(1)}, bf16[256,2048]{1,0:T(8,128)(2,1)}, u32[]{:S(2)}) copy-start(bf16[256,2048]{1,0:T(8,128)(2,1)} %reduce-scatter.3.cloned.1.call-done) | copy-start | bytes 3145732
Sparse Core Ops, SparseCore 0:
  9.5 49.3 all-gather.16
  60.4 34.2 all-gather.8
  96.9 49.0 all-gather.12
  148.0 38.7 all-gather.14
  188.8 47.7 all-gather.10
  248.7 43.1 reduce-scatter.2
  294.0 124.4 all-gather.20
  420.6 123.1 all-gather.22
  545.3 32.6 all-gather.18
  603.5 44.5 reduce-scatter.4
